TPU v7x, 32 devices: a whole 2x2x4 slice. The times are simulated.
32 devices in a mesh: fs: 16 (over z, y, x), tp: 2 (over core).
Axes of the slice: x: 2, y: 2, z: 4, core: 2. Of those that a mesh axis runs over, the one named last changes fastest.
Arguments:
- tokens: bfloat16 [6144, 2048], P('fs', 'tp'), may hold values from -24 to 24
- mixer_gain: float32 [2048], replicated, may hold values from 0.1 to 1.9
- pool_input: bfloat16 [2048, 1024], P('fs', 'tp'), may hold values from -0.125 to 0.125
- group_weight: bfloat16 [8, 128, 128], P('tp'), may hold values from -0.5 to 0.5
- channel_scale: float32 [1024], P('tp'), may hold values from 0.5 to 2
- pool_output: bfloat16 [1024, 2048], P('tp', 'fs'), may hold values from -0.1875 to 0.1875
- ffn_gain: float32 [2048], replicated, may hold values from 0.1 to 1.9
- gate_weight: bfloat16 [2048, 5632], P('fs', 'tp'), may hold values from -0.125 to 0.125
- up_weight: bfloat16 [2048, 5632], P('fs', 'tp'), may hold values from -0.125 to 0.125
- down_weight: bfloat16 [5632, 2048], P('tp', 'fs'), may hold values from -0.078125 to 0.078125
- final_gain: float32 [2048], P('tp'), may hold values from 0.1 to 1.9
Outputs:
- normed_out: bfloat16 [6144, 2048], P('fs', 'tp')
All inputs are finite; a program needn't handle non-finite values.
Results may differ from a plain program's by a relative error of at most 0.015.
Values may be sent and summed in bfloat16 or wider, within the bound.
No kernel may reach another device: no remote copies, remote signals or barrier semaphores. Data moves between devices by JAX's collectives and lax.ppermute only.
A program may use at most 128 MiB of HBM per device.

v0:
```python
import jax
import jax.numpy as jnp
from jax import lax
from jax.sharding import PartitionSpec as P

D = 2048
GROUP_DIM = 128
LENGTH = 128
EPS = 1e-06


def rms(values, gain):
    wide = values.astype(jnp.float32)
    scaled = wide * lax.rsqrt(jnp.mean(wide * wide, axis=-1, keepdims=True) + EPS)
    return scaled * gain


def add_rows(left, piece):
    return jnp.dot(left, piece, preferred_element_type=jnp.float32)


def local(
    tokens,
    mixer_gain,
    pool_input,
    group_weight,
    channel_scale,
    pool_output,
    ffn_gain,
    gate_weight,
    up_weight,
    down_weight,
    final_gain,
):
    full_rows = lax.all_gather(tokens, "tp", axis=1, tiled=True)
    first_normed = rms(full_rows, mixer_gain).astype(jnp.bfloat16)
    row_count = first_normed.shape[0]
    pooled_in = add_rows(first_normed, lax.all_gather(pool_input, "fs", axis=0, tiled=True)).astype(
        jnp.bfloat16
    )
    local_groups = group_weight.shape[0]
    group_ids = lax.axis_index("tp") * local_groups + jnp.arange(local_groups, dtype=jnp.int32)
    windows = jnp.left_shift(jnp.int32(2), group_ids % 4)
    later = jnp.arange(LENGTH, dtype=jnp.int32)[None, :, None]
    earlier = jnp.arange(LENGTH, dtype=jnp.int32)[None, None, :]
    reach = windows[:, None, None]
    inside = (earlier <= later) & (earlier > later - reach)
    band = inside.astype(jnp.bfloat16)
    divisor = jnp.minimum(later[:, :, 0] + 1, windows[:, None]).astype(jnp.float32)
    grid_low = pooled_in.reshape(row_count // LENGTH, LENGTH, local_groups, GROUP_DIM)
    window_sums = jnp.einsum("gts,nsgc->ntgc", band, grid_low, preferred_element_type=jnp.float32)
    average = window_sums / jnp.transpose(divisor)[None, :, :, None]
    pooled = (
        (average - grid_low.astype(jnp.float32))
        .astype(jnp.bfloat16)
        .reshape(row_count, local_groups, GROUP_DIM)
    )
    mapped = jnp.einsum("ngc,gcd->ngd", pooled, group_weight, preferred_element_type=jnp.float32)
    grouped = (mapped.reshape(row_count, local_groups * GROUP_DIM) * channel_scale).astype(
        jnp.bfloat16
    )
    mixer_terms = jnp.dot(
        grouped,
        lax.all_gather(pool_output, "fs", axis=1, tiled=True),
        preferred_element_type=jnp.float32,
    )
    mixer_out = lax.psum_scatter(
        mixer_terms.astype(jnp.bfloat16), "tp", scatter_dimension=1, tiled=True
    ).astype(jnp.float32)
    middle = (tokens.astype(jnp.float32) + mixer_out).astype(jnp.bfloat16)
    middle_rows = lax.all_gather(middle, "tp", axis=1, tiled=True)
    second_normed = rms(middle_rows, ffn_gain).astype(jnp.bfloat16)
    gate = add_rows(second_normed, lax.all_gather(gate_weight, "fs", axis=0, tiled=True))
    upward = add_rows(second_normed, lax.all_gather(up_weight, "fs", axis=0, tiled=True))
    hidden = (jax.nn.silu(gate) * upward).astype(jnp.bfloat16)
    ffn_terms = jnp.dot(
        hidden,
        lax.all_gather(down_weight, "fs", axis=1, tiled=True),
        preferred_element_type=jnp.float32,
    )
    ffn_out = lax.psum_scatter(
        ffn_terms.astype(jnp.bfloat16), "tp", scatter_dimension=1, tiled=True
    ).astype(jnp.float32)
    closing = middle.astype(jnp.float32) + ffn_out
    squares = lax.psum(jnp.sum(closing * closing, axis=1, keepdims=True), "tp")
    scaled = closing * lax.rsqrt(squares / D + EPS) * final_gain
    return scaled.astype(jnp.bfloat16)


def solution(mesh):
    placed = (
        P("fs", "tp"),
        P(),
        P("fs", "tp"),
        P("tp", None, None),
        P("tp"),
        P("tp", "fs"),
        P(),
        P("fs", "tp"),
        P("fs", "tp"),
        P("tp", "fs"),
        P("tp"),
    )
    return jax.shard_map(
        local, mesh=mesh, in_specs=placed, out_specs=P("fs", "tp"), check_vma=False
    )
```

profile of v0, /device:TPU:0, one launch (start us, length us, event | category | flops | bytes accessed | tf_op | source)
XLA Modules:
  0.0 684.9 jit_solution(15526173825975011963)
XLA Ops:
  6.5 0.7 all-gather.8.cloned.1.call-update
  7.3 0.7 all-gather.10.cloned.1.call-update
  8.1 0.7 all-gather.12.cloned.1.call-update
  9.0 12.4 %all-gather.8.cloned.1.call-done = bf16[384,2048]{1,0:T(8,128)(2,1)} async-done(((bf16[384,1024]{1,0:T(8,128)(2,1)}), bf16[384,2048]{1,0:T(8,128)(2,1)}) %all-gather.8.cloned.1.call-update) | async-done | bytes 1572880 | tf_op jit(solution)/shard_map/all_gather | solution.py:35
  21.4 1.8 fusion.1
  23.2 62.6 %all-gather.10.cloned.1.call-done = bf16[2048,512]{1,0:T(8,128)(2,1)} async-done(((bf16[128,512]{1,0:T(8,128)(2,1)}), bf16[2048,512]{1,0:T(8,128)(2,1)}) %all-gather.10.cloned.1.call-update) | async-done | bytes 2097168 | tf_op jit(solution)/shard_map/all_gather | solution.py:38
  85.8 3.1 fusion.14
  89.8 60.4 %all-gather.12.cloned.1.call-done = bf16[512,2048]{1,0:T(8,128)(2,1)} async-done(((bf16[512,128]{1,0:T(8,128)(2,1)}), bf16[512,2048]{1,0:T(8,128)(2,1)}) %all-gather.12.cloned.1.call-update) | async-done | bytes 2097168 | tf_op jit(solution)/shard_map/all_gather | solution.py:64
  150.3 3.8 convolution_convert_fusion.1
  154.1 7.2 %reduce-scatter.3.cloned.1.call-done = bf16[384,1024]{1,0:T(8,128)(2,1)} async-done(((bf16[384,2048]{1,0:T(8,128)(2,1)}), bf16[384,1024]{1,0:T(8,128)(2,1)}) %reduce-scatter.3.cloned.1.call-update) | async-done | bytes 786448 | tf_op jit(solution)/shard_map/reduce_scatter | solution.py:67
  161.4 2.3 add_convert_fusion
  164.3 0.7 all-gather.18.cloned.1.call-update
  165.1 0.7 all-gather.20.cloned.1.call-update
  166.0 8.9 %all-gather.14.cloned.1.call-done = bf16[384,2048]{1,0:T(8,128)(2,1)} async-done(((bf16[384,1024]{1,0:T(8,128)(2,1)}), bf16[384,2048]{1,0:T(8,128)(2,1)}) %all-gather.14.cloned.1.call-update) | async-done | bytes 1572880 | tf_op jit(solution)/shard_map/all_gather | solution.py:71
  174.9 1.8 fusion.4
  176.7 143.4 %all-gather.16.cloned.1.call-done = bf16[2048,2816]{1,0:T(8,128)(2,1)} async-done(((bf16[128,2816]{1,0:T(8,128)(2,1)}), bf16[2048,2816]{1,0:T(8,128)(2,1)}) %all-gather.16.cloned.1.call-update) | async-done | bytes 11534352 | tf_op jit(solution)/shard_map/all_gather | solution.py:73
  320.2 11.5 %fusion.20 = f32[384,2816]{1,0:T(8,128)} fusion(bf16[2048,2816]{1,0:T(8,128)(2,1)} %all-gather.16.cloned.1.call-done, bf16[384,2048]{1,0:T(8,128)(2,1)} %all-gather.14.cloned.1.call-done, f32[2048]{0:T(1024)S(1)} %copy-done.6, f32[384]{0:T(512)S(1)} %add_rsqrt_fusion), kind=kOutput, calls=%fused_computation.28 | convolution fusion | flops 4432330752 | bytes 17442304 | tf_op jit(solution)/shard_map/dot_general | solution.py:19
  331.7 130.8 %all-gather.18.cloned.1.call-done = bf16[2048,2816]{1,0:T(8,128)(2,1)} async-done(((bf16[128,2816]{1,0:T(8,128)(2,1)}), bf16[2048,2816]{1,0:T(8,128)(2,1)}) %all-gather.18.cloned.1.call-update) | async-done | bytes 11534352 | tf_op jit(solution)/shard_map/all_gather | solution.py:74
  462.5 183.0 %all-gather.20.cloned.1.call-done = bf16[2816,2048]{1,0:T(8,128)(2,1)} async-done(((bf16[2816,128]{1,0:T(8,128)(2,1)}), bf16[2816,2048]{1,0:T(8,128)(2,1)}) %all-gather.20.cloned.1.call-update) | async-done | bytes 11534352 | tf_op jit(solution)/shard_map/all_gather | solution.py:78
  645.5 19.3 %convolution_convert_fusion = bf16[384,2048]{1,0:T(8,128)(2,1)} fusion(bf16[2816,2048]{1,0:T(8,128)(2,1)} %all-gather.20.cloned.1.call-done, bf16[2048,2816]{1,0:T(8,128)(2,1)} %all-gather.18.cloned.1.call-done, f32[384,2816]{1,0:T(8,128)} %fusion.20, bf16[384,2048]{1,0:T(8,128)(2,1)S(1)} %copy-done.3, f32[2048]{0:T(1024)S(1)} %copy-done.6, ...), kind=kOutput, calls=%fused_computation.12 | convolution fusion | flops 8868790272 | bytes 30549504 | tf_op jit(solution)/shard_map/dot_general | solution.py:76
  664.8 7.3 %reduce-scatter.5.cloned.1.call-done = bf16[384,1024]{1,0:T(8,128)(2,1)} async-done(((bf16[384,2048]{1,0:T(8,128)(2,1)}), bf16[384,1024]{1,0:T(8,128)(2,1)}) %reduce-scatter.5.cloned.1.call-update) | async-done | bytes 786448 | tf_op jit(solution)/shard_map/reduce_scatter | solution.py:81
  672.1 1.5 multiply_reduce_fusion
  673.6 2.5 psum.7
  676.1 2.3 multiply_convert_fusion
  (40 shorter events, 2.2 us)
Async XLA Ops:
  6.5 82.8 %copy-start = (bf16[4,128,128]{2,1,0:T(8,128)(2,1)S(1)}, bf16[4,128,128]{2,1,0:T(8,128)(2,1)}, u32[]{:S(2)}) copy-start(bf16[4,128,128]{2,1,0:T(8,128)(2,1)} %param.14) | copy-start | bytes 393220
  6.5 14.9 %all-gather.8.cloned.1.call-start = ((), (), s32[]{:S(2)}) async-start(), calls=%async_computation.2 | async-start | bytes 2359296 | tf_op jit(solution)/shard_map/all_gather | solution.py:35
  7.3 78.5 %all-gather.10.cloned.1.call-start = ((), (), s32[]{:S(2)}) async-start(), calls=%async_computation.3 | async-start | bytes 2228224 | tf_op jit(solution)/shard_map/all_gather | solution.py:38
  8.0 142.3 %all-gather.12.cloned.1.call-start = ((), (), s32[]{:S(2)}) async-start(), calls=%async_computation.4 | async-start | bytes 2228224 | tf_op jit(solution)/shard_map/all_gather | solution.py:64
  8.7 152.6 %reduce-scatter.3.cloned.1.call-start = ((), (), s32[]{:S(2)}) async-start(), calls=%async_computation.5 | async-start | bytes 2359296 | tf_op jit(solution)/shard_map/reduce_scatter | solution.py:67
  88.9 0.8 copy-start.5
  89.7 71.7 %copy-start.2 = (bf16[384,1024]{1,0:T(8,128)(2,1)S(1)}, bf16[384,1024]{1,0:T(8,128)(2,1)}, u32[]{:S(2)}) copy-start(bf16[384,1024]{1,0:T(8,128)(2,1)} %param.11) | copy-start | bytes 2359300
  154.1 166.1 %copy-start.6 = (f32[2048]{0:T(1024)S(1)}, f32[2048]{0:T(1024)}, u32[]{:S(2)}) copy-start(f32[2048]{0:T(1024)} %param.17) | copy-start | bytes 24580
  154.1 20.8 %all-gather.14.cloned.1.call-start = ((), (), s32[]{:S(2)}) async-start(), calls=%async_computation.6 | async-start | bytes 2359296 | tf_op jit(solution)/shard_map/all_gather | solution.py:71
  163.7 156.5 %all-gather.16.cloned.1.call-start = ((), (), s32[]{:S(2)}) async-start(), calls=%async_computation.7 | async-start | bytes 12255232 | tf_op jit(solution)/shard_map/all_gather | solution.py:73
  164.3 298.3 %all-gather.18.cloned.1.call-start = ((), (), s32[]{:S(2)}) async-start(), calls=%async_computation.8 | async-start | bytes 12255232 | tf_op jit(solution)/shard_map/all_gather | solution.py:74
  165.0 480.5 %all-gather.20.cloned.1.call-start = ((), (), s32[]{:S(2)}) async-start(), calls=%async_computation.9 | async-start | bytes 12255232 | tf_op jit(solution)/shard_map/all_gather | solution.py:78
  165.8 506.3 %reduce-scatter.5.cloned.1.call-start = ((), (), s32[]{:S(2)}) async-start(), calls=%async_computation.10 | async-start | bytes 2359296 | tf_op jit(solution)/shard_map/reduce_scatter | solution.py:81
  176.7 468.8 %copy-start.3 = (bf16[384,2048]{1,0:T(8,128)(2,1)S(1)}, bf16[384,2048]{1,0:T(8,128)(2,1)}, u32[]{:S(2)}) copy-start(bf16[384,2048]{1,0:T(8,128)(2,1)} %all-gather.14.cloned.1.call-done) | copy-start | bytes 4718596
  331.7 340.4 %copy-start.1 = (bf16[384,1024]{1,0:T(8,128)(2,1)S(1)}, bf16[384,1024]{1,0:T(8,128)(2,1)}, u32[]{:S(2)}) copy-start(bf16[384,1024]{1,0:T(8,128)(2,1)} %add_convert_fusion) | copy-start | bytes 2359300
  664.8 11.3 %copy-start.4 = (f32[1024]{0:T(1024)S(1)}, f32[1024]{0:T(1024)}, u32[]{:S(2)}) copy-start(f32[1024]{0:T(1024)} %param.21) | copy-start | bytes 12292
Sparse Core Ops, SparseCore 0:
  8.9 12.5 all-gather.7
  24.2 61.5 all-gather.9
  88.5 61.7 all-gather.11
  154.2 7.1 reduce-scatter.2
  163.8 11.0 all-gather.13
  177.5 142.5 all-gather.15
  322.9 139.5 all-gather.17
  465.3 180.2 all-gather.19
  664.9 7.1 reduce-scatter.4
where the time goes:
time: 685 us
  waiting for transfers between devices  620 us (91%)
  matrix products  38.3 us (6%)
  between operations  13.3 us (2%)
  other arithmetic  10 us (1%)
    all_gather x1, waiting for transfers between devices, local(): lax.all_gather(down_weight, 'fs', axis=1, tiled=True)  183 us
    all_gather x1, waiting for transfers between devices, local(): lax.all_gather(gate_weight, 'fs', axis=0, tiled=True)  143 us
    all_gather x1, waiting for transfers between devices, local(): lax.all_gather(up_weight, 'fs', axis=0, tiled=True)  131 us
    all_gather x1, waiting for transfers between devices, local(): lax.all_gather(pool_input, 'fs', axis=0, tiled=True)  62.6 us
    all_gather x1, waiting for transfers between devices, local(): lax.all_gather(pool_output, 'fs', axis=1, tiled=True)  60.4 us
    dot_general x1, matrix products, local(): jnp.dot(hidden, lax.all_gather(down_weight, 'fs', axis=1, tiled=True), pr...  19.3 us
    dot_general x2, matrix products, add_rows(): return jnp.dot(left, piece, preferred_element_type=jnp.float32)  14.6 us
  transfers between devices with their start and end apart: 9, of which 9 were waited for; matrix products, arithmetic and copies ran while one was open for 3% of the time, Pallas kernels for 0%

commit v1 on v0

--- a/solution.py
+++ b/solution.py
@@ -75,7 +75,7 @@
     hidden = (jax.nn.silu(gate) * upward).astype(jnp.bfloat16)
     ffn_terms = jnp.dot(
         hidden,
-        lax.all_gather(down_weight, "fs", axis=1, tiled=True),
+        jnp.concatenate(lax.all_gather(down_weight, axis_name="fs"), 1),
         preferred_element_type=jnp.float32,
     )
     ffn_out = lax.psum_scatter(

time: 685 us -> 647 us (0.945)
  waiting for transfers between devices: 620 us -> 566 us
  local copies, waits for them, and re-layouts: 0.13 us -> 15.5 us
    all_gather x1, waiting for transfers between devices: 183 us -> 143 us  [local(): lax.all_gather(down_weight, axis_name='fs')]
    all_gather x1, waiting for transfers between devices: 143 us -> 127 us  [local(): lax.all_gather(gate_weight, 'fs', axis=0, tiled=True)]
    reshape x0 -> x1, local copies, waits for them, and re-layouts: none -> 15.3 us  [local(): jnp.concatenate(lax.all_gather(down_weight, axis_name='fs'), 1)]
  transfers between devices with their start and end apart: 9 -> 9, of which waited for: 9 -> 9; matrix products, arithmetic and copies ran while one was open for 3% -> 5% of each run, Pallas kernels for 0% -> 0%
where the time goes in v1:
time: 647 us
  waiting for transfers between devices  566 us (87%)
  matrix products  38.7 us (6%)
  local copies, waits for them, and re-layouts  15.5 us (2%)
  between operations  13.3 us (2%)
  other arithmetic  10 us (2%)
    all_gather x1, waiting for transfers between devices, local(): lax.all_gather(down_weight, axis_name='fs')  143 us
    all_gather x1, waiting for transfers between devices, local(): lax.all_gather(up_weight, 'fs', axis=0, tiled=True)  133 us
    all_gather x1, waiting for transfers between devices, local(): lax.all_gather(gate_weight, 'fs', axis=0, tiled=True)  127 us
    all_gather x1, waiting for transfers between devices, local(): lax.all_gather(pool_input, 'fs', axis=0, tiled=True)  62.6 us
    all_gather x1, waiting for transfers between devices, local(): lax.all_gather(pool_output, 'fs', axis=1, tiled=True)  60.4 us
    dot_general x1, matrix products, local(): jnp.dot(hidden, jnp.concatenate(lax.all_gather(down_weight, axis_name='fs...  21.5 us
    reshape x1, local copies, waits for them, and re-layouts, local(): jnp.concatenate(lax.all_gather(down_weight, axis_name='fs'), 1)  15.3 us
  transfers between devices with their start and end apart: 9, of which 9 were waited for; matrix products, arithmetic and copies ran while one was open for 5% of the time, Pallas kernels for 0%

profile of v1, /device:TPU:0, one launch (start us, length us, event | category | flops | bytes accessed | tf_op | source)
XLA Modules:
  0.0 646.6 jit_solution(9722449035734698221)
XLA Ops:
  6.5 0.7 all-gather.9.cloned.1.call-update
  7.3 0.7 all-gather.11.cloned.1.call-update
  9.0 12.4 %all-gather.9.cloned.1.call-done = bf16[384,2048]{1,0:T(8,128)(2,1)} async-done(((bf16[384,1024]{1,0:T(8,128)(2,1)}), bf16[384,2048]{1,0:T(8,128)(2,1)}) %all-gather.9.cloned.1.call-update) | async-done | bytes 1572880 | tf_op jit(solution)/shard_map/all_gather | solution.py:35
  21.4 1.8 fusion.1
  23.2 62.6 %all-gather.11.cloned.1.call-done = bf16[2048,512]{1,0:T(8,128)(2,1)} async-done(((bf16[128,512]{1,0:T(8,128)(2,1)}), bf16[2048,512]{1,0:T(8,128)(2,1)}) %all-gather.11.cloned.1.call-update) | async-done | bytes 2097168 | tf_op jit(solution)/shard_map/all_gather | solution.py:38
  85.8 3.1 fusion.14
  89.8 60.4 %all-gather.13.cloned.1.call-done = bf16[512,2048]{1,0:T(8,128)(2,1)} async-done(((bf16[512,128]{1,0:T(8,128)(2,1)}), bf16[512,2048]{1,0:T(8,128)(2,1)}) %all-gather.13.cloned.1.call-update) | async-done | bytes 2097168 | tf_op jit(solution)/shard_map/all_gather | solution.py:64
  150.3 3.8 convolution_convert_fusion.1
  154.1 7.2 %reduce-scatter.3.cloned.1.call-done = bf16[384,1024]{1,0:T(8,128)(2,1)} async-done(((bf16[384,2048]{1,0:T(8,128)(2,1)}), bf16[384,1024]{1,0:T(8,128)(2,1)}) %reduce-scatter.3.cloned.1.call-update) | async-done | bytes 786448 | tf_op jit(solution)/shard_map/reduce_scatter | solution.py:67
  161.3 2.3 add_convert_fusion
  164.3 0.7 all-gather.17.cloned.1.call-update
  165.1 0.7 all-gather.19.cloned.1.call-update
  165.8 9.1 %all-gather.15.cloned.1.call-done = bf16[384,2048]{1,0:T(8,128)(2,1)} async-done(((bf16[384,1024]{1,0:T(8,128)(2,1)}), bf16[384,2048]{1,0:T(8,128)(2,1)}) %all-gather.15.cloned.1.call-update) | async-done | bytes 1572880 | tf_op jit(solution)/shard_map/all_gather | solution.py:71
  174.9 1.8 fusion.4
  176.7 143.4 %all-gather.21.cloned.1.call-done = bf16[45056,128]{1,0:T(8,128)(2,1)} async-done(((bf16[2816,128]{1,0:T(8,128)(2,1)}), bf16[45056,128]{1,0:T(8,128)(2,1)}) %all-gather.21.cloned.1.call-update) | async-done | bytes 11534352 | tf_op jit(solution)/shard_map/all_gather | solution.py:78
  320.2 15.3 %copy.21 = bf16[2816,16,128]{0,2,1:T(8,128)(2,1)} copy(bf16[2816,16,128]{2,0,1:T(8,128)(2,1)} %bitcast.32) | data formatting | bytes 23068672 | tf_op jit(solution)/shard_map/reshape | solution.py:78
  335.5 127.0 %all-gather.17.cloned.1.call-done = bf16[2048,2816]{1,0:T(8,128)(2,1)} async-done(((bf16[128,2816]{1,0:T(8,128)(2,1)}), bf16[2048,2816]{1,0:T(8,128)(2,1)}) %all-gather.17.cloned.1.call-update) | async-done | bytes 11534352 | tf_op jit(solution)/shard_map/all_gather | solution.py:73
  462.5 9.7 %fusion.20 = f32[384,2816]{1,0:T(8,128)} fusion(bf16[2048,2816]{1,0:T(8,128)(2,1)} %all-gather.17.cloned.1.call-done, bf16[384,2048]{1,0:T(8,128)(2,1)S(1)} %copy-done.4, f32[2048]{0:T(1024)S(1)} %copy-done.7, f32[384]{0:T(512)S(1)} %add_rsqrt_fusion), kind=kOutput, calls=%fused_computation.28 | convolution fusion | flops 4432330752 | bytes 17442304 | tf_op jit(solution)/shard_map/dot_general | solution.py:19
  472.2 132.7 %all-gather.19.cloned.1.call-done = bf16[2048,2816]{1,0:T(8,128)(2,1)} async-done(((bf16[128,2816]{1,0:T(8,128)(2,1)}), bf16[2048,2816]{1,0:T(8,128)(2,1)}) %all-gather.19.cloned.1.call-update) | async-done | bytes 11534352 | tf_op jit(solution)/shard_map/all_gather | solution.py:74
  604.9 21.5 %convolution_convert_fusion = bf16[384,2048]{1,0:T(8,128)(2,1)} fusion(bf16[2816,2048]{0,1:T(8,128)(2,1)} %bitcast.33, bf16[2048,2816]{1,0:T(8,128)(2,1)} %all-gather.19.cloned.1.call-done, f32[384,2816]{1,0:T(8,128)} %fusion.20, bf16[384,2048]{1,0:T(8,128)(2,1)S(1)} %copy-done.4, f32[2048]{0:T(1024)S(1)} %copy-done.7, f32[384]{0:T(512)S(1)} %add_rsqrt_fusion), kind=kOutput, calls=%fused_computation.12 | convolution fusion | flops 8868790272 | bytes 30549504 | tf_op jit(solution)/shard_map/dot_general | solution.py:76
  626.5 7.3 %reduce-scatter.5.cloned.1.call-done = bf16[384,1024]{1,0:T(8,128)(2,1)} async-done(((bf16[384,2048]{1,0:T(8,128)(2,1)}), bf16[384,1024]{1,0:T(8,128)(2,1)}) %reduce-scatter.5.cloned.1.call-update) | async-done | bytes 786448 | tf_op jit(solution)/shard_map/reduce_scatter | solution.py:81
  633.8 1.5 multiply_reduce_fusion
  635.2 2.5 psum.7
  637.7 2.3 multiply_convert_fusion
  (43 shorter events, 2.7 us)
Async XLA Ops:
  6.5 82.8 %copy-start = (bf16[4,128,128]{2,1,0:T(8,128)(2,1)S(1)}, bf16[4,128,128]{2,1,0:T(8,128)(2,1)}, u32[]{:S(2)}) copy-start(bf16[4,128,128]{2,1,0:T(8,128)(2,1)} %param.14) | copy-start | bytes 393220
  6.5 14.9 %all-gather.9.cloned.1.call-start = ((), (), s32[]{:S(2)}) async-start(), calls=%async_computation.2 | async-start | bytes 2359296 | tf_op jit(solution)/shard_map/all_gather | solution.py:35
  7.3 78.5 %all-gather.11.cloned.1.call-start = ((), (), s32[]{:S(2)}) async-start(), calls=%async_computation.3 | async-start | bytes 2228224 | tf_op jit(solution)/shard_map/all_gather | solution.py:38
  8.0 142.3 %all-gather.13.cloned.1.call-start = ((), (), s32[]{:S(2)}) async-start(), calls=%async_computation.4 | async-start | bytes 2228224 | tf_op jit(solution)/shard_map/all_gather | solution.py:64
  8.7 152.6 %reduce-scatter.3.cloned.1.call-start = ((), (), s32[]{:S(2)}) async-start(), calls=%async_computation.5 | async-start | bytes 2359296 | tf_op jit(solution)/shard_map/reduce_scatter | solution.py:67
  88.9 0.8 copy-start.6
  89.7 71.7 %copy-start.3 = (bf16[384,1024]{1,0:T(8,128)(2,1)S(1)}, bf16[384,1024]{1,0:T(8,128)(2,1)}, u32[]{:S(2)}) copy-start(bf16[384,1024]{1,0:T(8,128)(2,1)} %param.11) | copy-start | bytes 2359300
  154.1 20.9 %all-gather.15.cloned.1.call-start = ((), (), s32[]{:S(2)}) async-start(), calls=%async_computation.6 | async-start | bytes 2359296 | tf_op jit(solution)/shard_map/all_gather | solution.py:71
  163.7 156.5 %all-gather.21.cloned.1.call-start = ((), (), s32[]{:S(2)}) async-start(), calls=%async_computation.10 | async-start | bytes 12255232 | tf_op jit(solution)/shard_map/all_gather | solution.py:78
  164.3 298.3 %all-gather.17.cloned.1.call-start = ((), (), s32[]{:S(2)}) async-start(), calls=%async_computation.7 | async-start | bytes 12255232 | tf_op jit(solution)/shard_map/all_gather | solution.py:73
  165.0 439.9 %all-gather.19.cloned.1.call-start = ((), (), s32[]{:S(2)}) async-start(), calls=%async_computation.8 | async-start | bytes 12255232 | tf_op jit(solution)/shard_map/all_gather | solution.py:74
  165.8 468.0 %reduce-scatter.5.cloned.1.call-start = ((), (), s32[]{:S(2)}) async-start(), calls=%async_computation.9 | async-start | bytes 2359296 | tf_op jit(solution)/shard_map/reduce_scatter | solution.py:81
  320.2 142.4 %copy-start.4 = (bf16[384,2048]{1,0:T(8,128)(2,1)S(1)}, bf16[384,2048]{1,0:T(8,128)(2,1)}, u32[]{:S(2)}) copy-start(bf16[384,2048]{1,0:T(8,128)(2,1)} %all-gather.15.cloned.1.call-done) | copy-start | bytes 4718596
  320.2 142.4 %copy-start.7 = (f32[2048]{0:T(1024)S(1)}, f32[2048]{0:T(1024)}, u32[]{:S(2)}) copy-start(f32[2048]{0:T(1024)} %param.17) | copy-start | bytes 24580
  604.9 28.8 %copy-start.2 = (bf16[384,1024]{1,0:T(8,128)(2,1)S(1)}, bf16[384,1024]{1,0:T(8,128)(2,1)}, u32[]{:S(2)}) copy-start(bf16[384,1024]{1,0:T(8,128)(2,1)} %add_convert_fusion) | copy-start | bytes 2359300
  604.9 35.1 %copy-start.1 = (bf16[4,128,128]{2,1,0:T(8,128)(2,1)S(1)}, bf16[4,128,128]{2,1,0:T(8,128)(2,1)}, u32[]{:S(2)}) copy-start(bf16[4,128,128]{2,1,0:T(8,128)(2,1)} %param.14) | copy-start | bytes 393220
  626.4 11.3 %copy-start.5 = (f32[1024]{0:T(1024)S(1)}, f32[1024]{0:T(1024)}, u32[]{:S(2)}) copy-start(f32[1024]{0:T(1024)} %param.21) | copy-start | bytes 12292
Sparse Core Ops, SparseCore 0:
  8.9 12.5 all-gather.8
  24.2 61.5 all-gather.10
  88.5 61.7 all-gather.12
  154.2 7.1 reduce-scatter.2
  163.8 11.0 all-gather.14
  177.5 142.5 all-gather.20
  322.9 139.5 all-gather.16
  465.3 139.5 all-gather.18
  626.6 7.1 reduce-scatter.4
